TPU v7x, 128 devices: a whole 4x4x4 slice. The times are simulated.
128 devices in a mesh: sp: 16 (over z, x), dp: 8 (over y, core).
Axes of the slice: x: 4, y: 4, z: 4, core: 2. Of those that a mesh axis runs over, the one named last changes fastest.
Arguments:
- resid: bfloat16 [8, 2048, 2048], P('dp', 'sp'), may hold values from -6 to 6
- queries: bfloat16 [8, 2048, 2048], P('dp', 'sp'), may hold values from -7 to 7
- keys: bfloat16 [8, 2048, 2048], P('dp', 'sp'), may hold values from -7 to 7
- values: bfloat16 [8, 2048, 2048], P('dp', 'sp'), may hold values from -6 to 6
- forget_cache: float32 [8, 32, 2048], P('dp', 'sp'), may hold values from -259 to 0, as said below
- query_gain: float32 [64], replicated, may hold values from 0.5 to 8
- key_gain: float32 [64], replicated, may hold values from 0.5 to 8
- out_weight: bfloat16 [2048, 2048], P(None, 'dp'), may hold values from -0.125 to 0.125
- norm_gain: float32 [2048], replicated, may hold values from 0.1 to 1.9
- routes: int32 [8, 2048, 2], P('dp', 'sp'), may hold values from 0 to 127, all different within a row; in each aligned block of 128 rows (0 to 127, 128 to 255, ..., all dimensions but the last counted through in order) at most 4 rows name the same one
- group_weight: float32 [8, 2048], P('dp', 'sp'), may hold values from 0.2 to 1
- inner_share: float32 [8, 2048, 2], P('dp', 'sp'), may hold values from 0.1 to 1
- expert_gate: bfloat16 [128, 2048, 1024], P(('sp', 'dp')), may hold values from -0.125 to 0.125
- expert_up: bfloat16 [128, 2048, 1024], P(('sp', 'dp')), may hold values from -0.125 to 0.125
- expert_down: bfloat16 [128, 1024, 2048], P(('sp', 'dp')), may hold values from -0.1875 to 0.1875
Outputs:
- layer_out: bfloat16 [8, 2048, 2048], P('dp', 'sp')
Inputs may be any that keep to these rules, and one draw needn't show every extreme that they name: `routes`: each row names 2 different experts; the rows of one device name one expert at most 4 times, a bound that some block reaches. `forget_cache`: along positions each head's values never rise.
All inputs are finite; a program needn't handle non-finite values.
Results may differ from a plain program's by a relative error of at most 0.0095.
The roundings to bfloat16 on the way count: a program that leaves them out, or rounds other values in their place, can miss the bound.
Values may be sent and summed in bfloat16 or wider, within the bound.
A program may use at most 128 MiB of HBM per device.

v0:
```python
import jax
import jax.numpy as jnp
from jax import lax
from jax.sharding import PartitionSpec as P

EPS = 1e-06


def side_by_side(arrays, axis, split_dim, concat_dim, along):
    both = jnp.concatenate(arrays, axis=along)
    out, at, finished = (
        lax.all_to_all(both, axis, split_axis=split_dim, concat_axis=concat_dim, tiled=True),
        0,
        [],
    )
    for a in arrays:
        finished.append(lax.slice_in_dim(out, at, at + a.shape[along], axis=along))
        at += a.shape[along]
    return tuple(finished)


def norm_rows(inputs, gain):
    floats = inputs.astype(jnp.float32)
    scaled = floats * lax.rsqrt(jnp.mean(floats * floats, axis=-1, keepdims=True) + EPS)
    return (scaled * gain).astype(jnp.bfloat16)


def shards(
    resid,
    queries,
    keys,
    values,
    forget_cache,
    query_gain,
    key_gain,
    out_weight,
    norm_gain,
    routes,
    group_weight,
    inner_share,
    expert_gate,
    expert_up,
    expert_down,
):
    head_q, head_k, head_v = side_by_side((queries, keys, values), "sp", 2, 1, 0)
    length = head_q.shape[1]
    local_heads = forget_cache.shape[1]
    head_size = query_gain.shape[0]
    query_normed = norm_rows(head_q[0].reshape(length, local_heads, head_size), query_gain)
    key_normed = norm_rows(head_k[0].reshape(length, local_heads, head_size), key_gain)
    value_rows = head_v[0].reshape(length, local_heads, head_size)
    cumulative = forget_cache[0]
    span = 512
    scale = head_size ** (-0.5)
    key_place = jnp.arange(length, dtype=jnp.int32)

    def attend(block_index):
        first = block_index * span
        query_block = lax.dynamic_slice_in_dim(query_normed, first, span, 0)
        query_decay = lax.dynamic_slice_in_dim(cumulative, first, span, 1)
        scores = (
            jnp.einsum("qhd,khd->hqk", query_block, key_normed, preferred_element_type=jnp.float32)
            * scale
        )
        scores = scores + query_decay[:, :, None] - cumulative[:, None, :]
        query_place = first + jnp.arange(span, dtype=jnp.int32)
        scores = jnp.where(key_place[None, None, :] <= query_place[None, :, None], scores, -jnp.inf)
        highest = jnp.max(scores, axis=-1, keepdims=True)
        expd = jnp.exp(scores - highest)
        probs = (expd / jnp.sum(expd, axis=-1, keepdims=True)).astype(jnp.bfloat16)
        return jnp.einsum(
            "hqk,khd->qhd", probs, value_rows, preferred_element_type=jnp.float32
        ).astype(jnp.bfloat16)

    blocks = lax.map(attend, jnp.arange(length // span, dtype=jnp.int32))
    head_out = blocks.reshape(1, length, local_heads * head_size)
    token_attn = lax.all_to_all(head_out, "sp", split_axis=1, concat_axis=2, tiled=True)[0]
    projected = jnp.dot(
        token_attn,
        lax.all_gather(out_weight, "dp", axis=1, tiled=True),
        preferred_element_type=jnp.float32,
    )
    mid = (resid[0].astype(jnp.float32) + projected).astype(jnp.bfloat16)
    normed = norm_rows(mid, norm_gain)
    width = normed.shape[1]
    tok_count = normed.shape[0]
    top_count = routes.shape[2]
    experts = lax.axis_size("sp") * lax.axis_size("dp")
    capacity = 2 * tok_count * top_count // experts
    expert_ids = routes[0].reshape(-1)
    expert_onehot = (expert_ids[:, None] == jnp.arange(experts, dtype=jnp.int32)[None, :]).astype(
        jnp.int32
    )
    earlier = jnp.cumsum(expert_onehot, axis=0) - expert_onehot
    slot_rank = jnp.sum(earlier * expert_onehot, axis=1)
    slot_index = (expert_ids * capacity + slot_rank).reshape(tok_count, top_count)
    slot_range = jnp.arange(experts * capacity, dtype=jnp.int32)
    dispatch = jnp.any(slot_range[:, None, None] == slot_index[None, :, :], axis=2).astype(
        jnp.bfloat16
    )
    send = jnp.dot(dispatch, normed, preferred_element_type=jnp.float32).astype(jnp.bfloat16)
    arrived = lax.all_to_all(
        send.reshape(experts, capacity, width),
        ("sp", "dp"),
        split_axis=0,
        concat_axis=0,
        tiled=True,
    )
    flat_rows = arrived.reshape(-1, width)
    gate = jnp.dot(flat_rows, expert_gate[0], preferred_element_type=jnp.float32)
    upper = jnp.dot(flat_rows, expert_up[0], preferred_element_type=jnp.float32)
    hidden = (jax.nn.silu(gate) * upper).astype(jnp.bfloat16)
    result = jnp.dot(hidden, expert_down[0], preferred_element_type=jnp.float32).astype(
        jnp.bfloat16
    )
    returned = lax.all_to_all(
        result.reshape(arrived.shape), ("sp", "dp"), split_axis=0, concat_axis=0, tiled=True
    )
    returned = returned.reshape(experts * capacity, width)
    shares = inner_share[0]
    weights = group_weight[0][:, None] * shares / jnp.sum(shares, axis=-1, keepdims=True)
    mixed = jnp.zeros((tok_count, width), jnp.float32)
    for route in range(top_count):
        select = (slot_range[None, :] == slot_index[:, route : route + 1]).astype(jnp.bfloat16)
        picked = jnp.dot(select, returned, preferred_element_type=jnp.float32)
        mixed = mixed + weights[:, route : route + 1] * picked
    layer_out = (mid.astype(jnp.float32) + mixed).astype(jnp.bfloat16)
    return layer_out.reshape(1, tok_count, width)


def solution(mesh):
    return jax.shard_map(
        shards,
        mesh=mesh,
        in_specs=(
            P("dp", "sp", None),
            P("dp", "sp", None),
            P("dp", "sp", None),
            P("dp", "sp", None),
            P("dp", "sp", None),
            P(),
            P(),
            P(None, "dp"),
            P(),
            P("dp", "sp", None),
            P("dp", "sp"),
            P("dp", "sp", None),
            P(("sp", "dp"), None, None),
            P(("sp", "dp"), None, None),
            P(("sp", "dp"), None, None),
        ),
        out_specs=P("dp", "sp", None),
        check_vma=False,
    )
```

profile of v0, /device:TPU:1, one launch (start us, length us, event | category | flops | bytes accessed | tf_op | source)
XLA Modules:
  0.0 254.3 jit_solution(731116394836500917)
XLA Ops:
  7.3 1.5 pad_maximum_fusion
  8.8 2.6 %copy.99 = bf16[3,128,2048]{1,0,2:T(4,128)(2,1)} copy(bf16[3,128,2048]{2,1,0:T(8,128)(2,1)S(1)} %pad_maximum_fusion) | data formatting | bytes 3145728 | tf_op jit(solution)/shard_map/concatenate | solution.py:10
  11.4 8.4 %all-to-all-start = ((bf16[3,128,2048]{1,0,2:T(4,128)(2,1)}), bf16[3,128,2048]{1,0,2:T(4,128)(2,1)S(1)}, u32[]{:S(2)}, u32[]{:S(2)}) async-start(bf16[3,128,2048]{1,0,2:T(4,128)(2,1)} %copy.99), calls=%async_computation | async-start | bytes 4194304 | tf_op jit(solution)/shard_map/all_to_all | solution.py:12
  20.5 30.3 %all-to-all-done = bf16[3,128,2048]{1,0,2:T(4,128)(2,1)S(1)} async-done(((bf16[3,128,2048]{1,0,2:T(4,128)(2,1)}), bf16[3,128,2048]{1,0,2:T(4,128)(2,1)S(1)}, u32[]{:S(2)}, u32[]{:S(2)}) %all-to-all-start) | async-done | bytes 1572896 | tf_op jit(solution)/shard_map/all_to_all | solution.py:12
  50.8 2.4 copy.101
  53.2 2.8 %fusion.70 = (bf16[1,16,128,128]{3,2,1,0:T(8,128)(2,1)}, f32[1,16,128,128]{3,2,1,0:T(8,128)S(1)}, f32[1,16,128,128]{3,2,1,0:T(8,128)}) fusion(bf16[3,16,128,128]{3,2,1,0:T(8,128)(2,1)} %bitcast.98), kind=kLoop, calls=%fused_computation.88 | loop fusion | flops 524288 | bytes 4194304 | tf_op jit(solution)/shard_map/slice | solution.py:17
  56.7 1.7 copy.102
  58.6 1.5 copy.104
  61.4 1.4 multiply_convert_fusion.2
  62.8 46.6 %while.11 = (s32[]{:T(128)}, bf16[4,512,2,64]{1,3,2,0:T(8,128)(2,1)S(1)}, s32[4]{0:T(128)S(1)}, bf16[2048,2,64]{0,2,1:T(8,128)(2,1)}, bf16[2048,2,64]{0,2,1:T(8,...) while((s32[]{:T(128)}, ...), condition=%wide.region_5.6_spmd.clone, body=%wide.region_2.5_spmd.clone.sunk | while | flops 833689088 | bytes 7271131 | solution.py:75
  64.8 4.7 %fusion.93 = f32[2,512]{1,0:T(2,128)S(1)} fusion(f32[2,2048]{1,0:T(2,128)S(1)} %bitcast.107, f32[2,512]{1,0:T(2,128)S(1)} %constant_dynamic-slice_fusion.2, pred[512,2048]{1,0:T(8,128)(4,1)S(1)} %iota_compare_fusion.8, bf16[2048,2,64]{0,2,1:T(8,128)(2,1)} %get-tuple-element.183, bf16[2048,2,64]{0,2,1:T(8,128)(2,1)} %get-tuple-element.182, ...), kind=kOutput, calls=%fused_computation.87.clone.1 | convolution fusion | flops 281020416 | bytes 1728516 | tf_op jit(solution)/shard_map/while/body/eval_jaxpr/sub | solution.py:69
  69.5 5.0 %fusion.94 = bf16[4,512,2,64]{1,3,2,0:T(8,128)(2,1)S(1)} fusion(bf16[4,512,2,64]{1,3,2,0:T(8,128)(2,1)S(1)} %get-tuple-element.168, s32[]{:T(128)} %get-tuple-element.167, bf16[2048,2,64]{0,2,1:T(8,128)(2,1)S(1)} %get-tuple-element.186, f32[2,512]{1,0:T(2,128)S(1)} %fusion.93, f32[2,2048]{1,0:T(2,128)S(1)} %bitcast.108, ...), kind=kOutput, calls=%fused_computation.16.clone.1 | convolution fusion | flops 551619584 | bytes 2384388 | tf_op jit(solution)/shard_map/while/body/eval_jaxpr/hqk,khd->qhd/dot_general | solution.py:71
  76.4 4.7 %fusion.93 = f32[2,512]{1,0:T(2,128)S(1)} fusion(f32[2,2048]{1,0:T(2,128)S(1)} %bitcast.107, f32[2,512]{1,0:T(2,128)S(1)} %constant_dynamic-slice_fusion.2, pred[512,2048]{1,0:T(8,128)(4,1)S(1)} %iota_compare_fusion.8, bf16[2048,2,64]{0,2,1:T(8,128)(2,1)} %get-tuple-element.183, bf16[2048,2,64]{0,2,1:T(8,128)(2,1)} %get-tuple-element.182, ...), kind=kOutput, calls=%fused_computation.87.clone.1 | convolution fusion | flops 281020416 | bytes 1728516 | tf_op jit(solution)/shard_map/while/body/eval_jaxpr/sub | solution.py:69
  81.1 5.0 %fusion.94 = bf16[4,512,2,64]{1,3,2,0:T(8,128)(2,1)S(1)} fusion(bf16[4,512,2,64]{1,3,2,0:T(8,128)(2,1)S(1)} %get-tuple-element.168, s32[]{:T(128)} %get-tuple-element.167, bf16[2048,2,64]{0,2,1:T(8,128)(2,1)S(1)} %get-tuple-element.186, f32[2,512]{1,0:T(2,128)S(1)} %fusion.93, f32[2,2048]{1,0:T(2,128)S(1)} %bitcast.108, ...), kind=kOutput, calls=%fused_computation.16.clone.1 | convolution fusion | flops 551619584 | bytes 2384388 | tf_op jit(solution)/shard_map/while/body/eval_jaxpr/hqk,khd->qhd/dot_general | solution.py:71
  88.1 4.7 %fusion.93 = f32[2,512]{1,0:T(2,128)S(1)} fusion(f32[2,2048]{1,0:T(2,128)S(1)} %bitcast.107, f32[2,512]{1,0:T(2,128)S(1)} %constant_dynamic-slice_fusion.2, pred[512,2048]{1,0:T(8,128)(4,1)S(1)} %iota_compare_fusion.8, bf16[2048,2,64]{0,2,1:T(8,128)(2,1)} %get-tuple-element.183, bf16[2048,2,64]{0,2,1:T(8,128)(2,1)} %get-tuple-element.182, ...), kind=kOutput, calls=%fused_computation.87.clone.1 | convolution fusion | flops 281020416 | bytes 1728516 | tf_op jit(solution)/shard_map/while/body/eval_jaxpr/sub | solution.py:69
  92.8 5.0 %fusion.94 = bf16[4,512,2,64]{1,3,2,0:T(8,128)(2,1)S(1)} fusion(bf16[4,512,2,64]{1,3,2,0:T(8,128)(2,1)S(1)} %get-tuple-element.168, s32[]{:T(128)} %get-tuple-element.167, bf16[2048,2,64]{0,2,1:T(8,128)(2,1)S(1)} %get-tuple-element.186, f32[2,512]{1,0:T(2,128)S(1)} %fusion.93, f32[2,2048]{1,0:T(2,128)S(1)} %bitcast.108, ...), kind=kOutput, calls=%fused_computation.16.clone.1 | convolution fusion | flops 551619584 | bytes 2384388 | tf_op jit(solution)/shard_map/while/body/eval_jaxpr/hqk,khd->qhd/dot_general | solution.py:71
  99.7 4.7 %fusion.93 = f32[2,512]{1,0:T(2,128)S(1)} fusion(f32[2,2048]{1,0:T(2,128)S(1)} %bitcast.107, f32[2,512]{1,0:T(2,128)S(1)} %constant_dynamic-slice_fusion.2, pred[512,2048]{1,0:T(8,128)(4,1)S(1)} %iota_compare_fusion.8, bf16[2048,2,64]{0,2,1:T(8,128)(2,1)} %get-tuple-element.183, bf16[2048,2,64]{0,2,1:T(8,128)(2,1)} %get-tuple-element.182, ...), kind=kOutput, calls=%fused_computation.87.clone.1 | convolution fusion | flops 281020416 | bytes 1728516 | tf_op jit(solution)/shard_map/while/body/eval_jaxpr/sub | solution.py:69
  104.4 5.0 %fusion.94 = bf16[4,512,2,64]{1,3,2,0:T(8,128)(2,1)S(1)} fusion(bf16[4,512,2,64]{1,3,2,0:T(8,128)(2,1)S(1)} %get-tuple-element.168, s32[]{:T(128)} %get-tuple-element.167, bf16[2048,2,64]{0,2,1:T(8,128)(2,1)S(1)} %get-tuple-element.186, f32[2,512]{1,0:T(2,128)S(1)} %fusion.93, f32[2,2048]{1,0:T(2,128)S(1)} %bitcast.108, ...), kind=kOutput, calls=%fused_computation.16.clone.1 | convolution fusion | flops 551619584 | bytes 2384388 | tf_op jit(solution)/shard_map/while/body/eval_jaxpr/hqk,khd->qhd/dot_general | solution.py:71
  111.4 11.8 %reduce.5 = bf16[2048,128]{1,0:T(8,128)(2,1)S(1)} reduce(bf16[2048,1,128]{2,1,0:T(2,128)(2,1)S(1)} %bitcast.100, bf16[]{:T(256)} %broadcast.121), dimensions={1}, to_apply=%bitcast.70.reduce_sub_computation | reduce | bytes 1048578
  124.1 4.3 %all-to-all-start.1 = ((bf16[16,2,8192]{2,1,0:T(2,128)(2,1)}), bf16[16,2,8192]{2,1,0:T(2,128)(2,1)S(1)}, u32[]{:S(2)}, u32[]{:S(2)}) async-start(bf16[16,2,8192]{2,1,0:T(2,128)(2,1)} %reshape.139), calls=%async_computation.1 | async-start | bytes 1048576 | tf_op jit(solution)/shard_map/all_to_all | solution.py:77
  129.1 9.6 %all-to-all-done.1 = bf16[16,2,8192]{2,1,0:T(2,128)(2,1)S(1)} async-done(((bf16[16,2,8192]{2,1,0:T(2,128)(2,1)}), bf16[16,2,8192]{2,1,0:T(2,128)(2,1)S(1)}, u32[]{:S(2)}, u32[]{:S(2)}) %all-to-all-start.1) | async-done | bytes 524320 | tf_op jit(solution)/shard_map/all_to_all | solution.py:77
  139.7 4.7 %multiply_reduce_fusion = (f32[128]{0:T(128)S(1)}, f32[128,2048]{1,0:T(8,128)S(1)}) fusion(bf16[128,2048]{0,1:T(8,128)(2,1)S(1)} %bitcast.101, bf16[2048,2048]{1,0:T(8,128)(2,1)} %all-gather.2.cloned.1.call-done, bf16[1,128,2048]{2,1,0:T(8,128)(2,1)S(1)} %copy-done.1), kind=kOutput, calls=%fused_computation.50 | convolution fusion | flops 1075314560 | bytes 10486272 | tf_op jit(solution)/shard_map/dot_general | solution.py:78
  145.2 2.2 reshape.128
  147.5 37.1 %all_to_all.40 = bf16[128,4,2048]{2,1,0:T(4,128)(2,1)S(1)} all-to-all(bf16[128,4,2048]{2,1,0:T(4,128)(2,1)} %reshape.128), channel_id=1, replica_groups=mesh['sp'=16,'dp'=8] {'sp','dp'}, dimensions={0} | all-to-all | bytes 4194304 | tf_op jit(solution)/shard_map/all_to_all | solution.py:102
  184.6 2.0 reshape.129
  186.6 6.6 %fusion.40 = f32[512,1024]{1,0:T(8,128)} fusion(bf16[512,2048]{1,0:T(8,128)(2,1)} %reshape.129, bf16[1,2048,1024]{2,1,0:T(8,128)(2,1)} %param.29), kind=kOutput, calls=%fused_computation.34 | convolution fusion | flops 2147483648 | bytes 8388608 | tf_op jit(solution)/shard_map/dot_general | solution.py:110
  193.3 9.9 %fusion.42 = bf16[512,2048]{1,0:T(8,128)(2,1)} fusion(bf16[1,1024,2048]{2,1,0:T(8,128)(2,1)} %param.31, f32[512,1024]{1,0:T(8,128)} %fusion.40, bf16[512,2048]{1,0:T(8,128)(2,1)S(1)} %copy-done, bf16[1,2048,1024]{2,1,0:T(8,128)(2,1)} %param.30), kind=kOutput, calls=%fused_computation.36 | convolution fusion | flops 4299161600 | bytes 14680064 | tf_op jit(solution)/shard_map/dot_general | solution.py:113
  203.2 4.1 %reshape.130 = bf16[128,4,2048]{2,1,0:T(4,128)(2,1)} reshape(bf16[512,2048]{1,0:T(8,128)(2,1)} %fusion.42) | data formatting | bytes 4194304 | tf_op jit(solution)/shard_map/reshape | solution.py:117
  207.3 5.8 %all-to-all-start.3 = ((bf16[128,4,2048]{2,1,0:T(4,128)(2,1)}), bf16[128,4,2048]{2,1,0:T(4,128)(2,1)}, u32[]{:S(2)}, u32[]{:S(2)}) async-start(bf16[128,4,2048]{2,1,0:T(4,128)(2,1)} %reshape.130), calls=%async_computation.3 | async-start | bytes 4194304 | tf_op jit(solution)/shard_map/all_to_all | solution.py:116
  213.5 29.5 %all-to-all-done.3 = bf16[128,4,2048]{2,1,0:T(4,128)(2,1)} async-done(((bf16[128,4,2048]{2,1,0:T(4,128)(2,1)}), bf16[128,4,2048]{2,1,0:T(4,128)(2,1)}, u32[]{:S(2)}, u32[]{:S(2)}) %all-to-all-start.3) | async-done | bytes 2097184 | tf_op jit(solution)/shard_map/all_to_all | solution.py:116
  243.0 2.5 reshape.131
  246.0 1.4 fusion.50
  (94 shorter events, 14.5 us)
Async XLA Ops:
  6.5 133.1 %all-gather.2.cloned.1.call-start = ((), (), s32[]{:S(2)}) async-start(), calls=%async_computation.4 | async-start | bytes 9437184 | tf_op jit(solution)/shard_map/all_gather | solution.py:80
  8.8 11.0 %copy-start.9 = (s32[1,128,2]{1,2,0:T(2,128)S(1)}, s32[1,128,2]{1,2,0:T(2,128)}, u32[]{:S(2)}) copy-start(s32[1,128,2]{1,2,0:T(2,128)} %param.26) | copy-start | bytes 3076
  11.4 39.4 %all-to-all-start = ((bf16[3,128,2048]{1,0,2:T(4,128)(2,1)}), bf16[3,128,2048]{1,0,2:T(4,128)(2,1)S(1)}, u32[]{:S(2)}, u32[]{:S(2)}) async-start(bf16[3,128,2048]{1,0,2:T(4,128)(2,1)} %copy.99), calls=%async_computation | async-start | bytes 4194304 | tf_op jit(solution)/shard_map/all_to_all | solution.py:12
  20.5 36.0 %copy-start.7 = (s32[128,3]{0,1:T(4,128)}, s32[128,3]{0,1:T(4,128)S(1)}, u32[]{:S(2)}) copy-start(s32[128,3]{0,1:T(4,128)S(1)} %reduce-window.9) | copy-start | bytes 4612
  56.6 4.8 %copy-start.10 = (f32[64]{0:T(128)S(1)}, f32[64]{0:T(128)}, u32[]{:S(2)}) copy-start(f32[64]{0:T(128)} %param.23) | copy-start | bytes 772
  56.6 4.8 %copy-start.11 = (f32[64]{0:T(128)S(1)}, f32[64]{0:T(128)}, u32[]{:S(2)}) copy-start(f32[64]{0:T(128)} %param.22) | copy-start | bytes 772
  58.6 4.2 %copy-start.2 = (bf16[4,512,2,64]{1,3,2,0:T(8,128)(2,1)S(1)}, bf16[4,512,2,64]{1,3,2,0:T(8,128)(2,1)}, u32[]{:S(2)}) copy-start(bf16[4,512,2,64]{1,3,2,0:T(8,128)(2,1)} %custom-call) | copy-start | bytes 1572868
  58.6 4.2 %copy-start.5 = (f32[1,2,2048]{2,1,0:T(2,128)S(1)}, f32[1,2,2048]{2,1,0:T(2,128)}, u32[]{:S(2)}) copy-start(f32[1,2,2048]{2,1,0:T(2,128)} %param.21) | copy-start | bytes 49156
  61.1 1.7 copy-start.3
  64.8 4.7 %copy-start.4 = (bf16[2048,2,64]{0,2,1:T(8,128)(2,1)S(1)}, bf16[2048,2,64]{0,2,1:T(8,128)(2,1)}, u32[]{:S(2)}) copy-start(bf16[2048,2,64]{0,2,1:T(8,128)(2,1)} %get-tuple-element.183) | copy-start | bytes 1572868 | tf_op jit(solution)/shard_map/while
  76.4 4.7 %copy-start.4 = (bf16[2048,2,64]{0,2,1:T(8,128)(2,1)S(1)}, bf16[2048,2,64]{0,2,1:T(8,128)(2,1)}, u32[]{:S(2)}) copy-start(bf16[2048,2,64]{0,2,1:T(8,128)(2,1)} %get-tuple-element.183) | copy-start | bytes 1572868 | tf_op jit(solution)/shard_map/while
  88.1 4.7 %copy-start.4 = (bf16[2048,2,64]{0,2,1:T(8,128)(2,1)S(1)}, bf16[2048,2,64]{0,2,1:T(8,128)(2,1)}, u32[]{:S(2)}) copy-start(bf16[2048,2,64]{0,2,1:T(8,128)(2,1)} %get-tuple-element.183) | copy-start | bytes 1572868 | tf_op jit(solution)/shard_map/while
  99.7 4.7 %copy-start.4 = (bf16[2048,2,64]{0,2,1:T(8,128)(2,1)S(1)}, bf16[2048,2,64]{0,2,1:T(8,128)(2,1)}, u32[]{:S(2)}) copy-start(bf16[2048,2,64]{0,2,1:T(8,128)(2,1)} %get-tuple-element.183) | copy-start | bytes 1572868 | tf_op jit(solution)/shard_map/while
  109.4 19.0 %slice-start = ((s32[128,3]{0,1:T(4,128)}), s32[128,2]{0,1:T(2,128)S(1)}, s32[]{:S(2)}) async-start(s32[128,3]{0,1:T(4,128)} %copy-done.7), calls=%async_computation.5 | async-start | bytes 2048 | tf_op jit(solution)/shard_map/slice.1
  111.4 28.3 %copy-start.1 = (bf16[1,128,2048]{2,1,0:T(8,128)(2,1)S(1)}, bf16[1,128,2048]{2,1,0:T(8,128)(2,1)}, u32[]{:S(2)}) copy-start(bf16[1,128,2048]{2,1,0:T(8,128)(2,1)} %param.17) | copy-start | bytes 1572868
  124.1 14.7 %all-to-all-start.1 = ((bf16[16,2,8192]{2,1,0:T(2,128)(2,1)}), bf16[16,2,8192]{2,1,0:T(2,128)(2,1)S(1)}, u32[]{:S(2)}, u32[]{:S(2)}) async-start(bf16[16,2,8192]{2,1,0:T(2,128)(2,1)} %reshape.139), calls=%async_computation.1 | async-start | bytes 1048576 | tf_op jit(solution)/shard_map/all_to_all | solution.py:77
  139.7 4.8 %copy-start.6 = (f32[2048]{0:T(1024)S(1)}, f32[2048]{0:T(1024)}, u32[]{:S(2)}) copy-start(f32[2048]{0:T(1024)} %param.25) | copy-start | bytes 24580
  186.6 6.7 %copy-start = (bf16[512,2048]{1,0:T(8,128)(2,1)S(1)}, bf16[512,2048]{1,0:T(8,128)(2,1)}, u32[]{:S(2)}) copy-start(bf16[512,2048]{1,0:T(8,128)(2,1)} %reshape.129) | copy-start | bytes 6291460
  203.2 10.1 %copy-start.8 = (f32[1,128,2]{1,2,0:T(2,128)S(1)}, f32[1,128,2]{1,2,0:T(2,128)}, u32[]{:S(2)}) copy-start(f32[1,128,2]{1,2,0:T(2,128)} %param.28) | copy-start | bytes 3076
  203.2 10.3 %copy-start.12 = (f32[1,128]{1,0:T(1,128)S(1)}, f32[1,128]{1,0:T(1,128)}, u32[]{:S(2)}) copy-start(f32[1,128]{1,0:T(1,128)} %param.27) | copy-start | bytes 1540
  207.3 35.7 %all-to-all-start.3 = ((bf16[128,4,2048]{2,1,0:T(4,128)(2,1)}), bf16[128,4,2048]{2,1,0:T(4,128)(2,1)}, u32[]{:S(2)}, u32[]{:S(2)}) async-start(bf16[128,4,2048]{2,1,0:T(4,128)(2,1)} %reshape.130), calls=%async_computation.3 | async-start | bytes 4194304 | tf_op jit(solution)/shard_map/all_to_all | solution.py:116
Sparse Core Ops, SparseCore 0:
  9.0 57.0 all-gather.1
where the time goes:
time: 255 us; the launch traced here: 254 us
  waiting for transfers between devices  70.2 us (28%)
  matrix products  62.7 us (25%)
  blocking collectives  37.1 us (15%)
  local copies, waits for them, and re-layouts  28.2 us (11%)
  other arithmetic  20.9 us (8%)
  starting transfers between devices  18.6 us (7%)
  between operations  13.8 us (5%)
  loops' own time  2.88 us (1%)
    all_to_all x1, blocking collectives, shards(): lax.all_to_all(send.reshape(experts, capacity, width), ('sp', 'dp'), spli...  37.1 us
    all_to_all x1, waiting for transfers between devices, side_by_side(): lax.all_to_all(both, axis, split_axis=split_dim, concat_axis=concat_dim,...  30.3 us
    all_to_all x1, waiting for transfers between devices, shards(): lax.all_to_all(result.reshape(arrived.shape), ('sp', 'dp'), split_axis=0,...  29.5 us
    dot_general x4, matrix products, attend(): jnp.einsum('hqk,khd->qhd', probs, value_rows, preferred_element_type=jnp....  19.9 us
    sub x4, matrix products, attend(): expd = jnp.exp(scores - highest)  18.8 us
    unnamed x1, other arithmetic  11.8 us
    dot_general x1, matrix products, shards(): jnp.dot(hidden, expert_down[0], preferred_element_type=jnp.float32)  9.89 us
    all_to_all x1, waiting for transfers between devices, shards(): lax.all_to_all(head_out, 'sp', split_axis=1, concat_axis=2, tiled=True)[0]  9.64 us
  transfers between devices with their start and end apart: 4, of which 3 were waited for; matrix products, arithmetic and copies ran while one was open for 30% of the time, Pallas kernels for 0%

commit v1 on v0

v1 whole, which is shorter than its diff:
```python
import functools

import jax
import jax.numpy as jnp
from jax import lax
from jax.experimental import pallas as pl
from jax.experimental.pallas import tpu as pltpu
from jax.sharding import PartitionSpec as P

EPS = 1e-06
MESH = pl.DeviceIdType.MESH
F32 = jnp.float32
BF16 = jnp.bfloat16
D = 2048
HD = 64
FF = 1024
TOK = 128
SEQ = 2048
QB = 256
MULT = 37
SP_MULT = 7


def dot(a, b):
    return jnp.dot(a, b, preferred_element_type=F32)


def drain(ref, sem):
    pltpu.make_async_copy(ref, ref, sem).wait()


def iota(shape, dim):
    return lax.broadcasted_iota(jnp.int32, shape, dim)


def mod(a, n):
    return lax.rem(a, n)


def kernel(
    q_h,
    k_h,
    v_h,
    resid_h,
    ow_h,
    eg_h,
    eu_h,
    ed_h,
    fc_ref,
    qg_ref,
    kg_ref,
    ng_ref,
    routes_ref,
    gw_ref,
    ish_ref,
    out_ref,
    qkv_s,
    qkv_r,
    qh,
    kt,
    ao,
    ar,
    wsrc,
    wr,
    psend,
    precv,
    resid_s,
    disp,
    pick,
    perm,
    wg,
    wu,
    wd,
    send,
    recv,
    ysend,
    ret,
    acc,
    wts,
    loc_sem,
    qkv_send,
    qkv_recv,
    w_send,
    w_near,
    w_far,
    w_part,
    a_send,
    a_recv,
    p_send,
    p_recv,
    d_send,
    d_recv,
    r_send,
    r_recv,
    ready,
):
    sp = lax.axis_index("sp")
    dp = lax.axis_index("dp")
    z, x = sp // 4, mod(sp, 4)
    y, c = dp // 2, mod(dp, 2)
    sign = 1 - 2 * c

    local = []
    for n, (src, dst) in enumerate(
        (
            (k_h, qkv_s.at[0]),
            (q_h, qkv_s.at[1]),
            (v_h, qkv_s.at[2]),
            (ow_h, wsrc),
            (ow_h.at[pl.ds(pl.multiple_of(c * 1024, 1024), 1024)],
             wr.at[:, pl.ds(pl.multiple_of(dp * 256, 256), 256)]),
            (resid_h, resid_s),
        )
    ):
        copy = pltpu.make_async_copy(src, dst, loc_sem.at[n])
        copy.start()
        local.append(copy)
    barrier = pltpu.get_barrier_semaphore()
    for k in range(1, 16):
        pl.semaphore_signal(barrier, inc=1, device_id=(mod(sp + k, 16), dp), device_id_type=MESH)
    for k in range(1, 8):
        pl.semaphore_signal(barrier, inc=1, device_id=(sp, mod(dp + k, 8)), device_id_type=MESH)
    pl.semaphore_wait(barrier, 22)

    def remote(src, dst, ssem, rsem, dev):
        return pltpu.make_async_remote_copy(
            src_ref=src, dst_ref=dst, send_sem=ssem, recv_sem=rsem, device_id=dev, device_id_type=MESH
        )

    my_rows = pl.ds(pl.multiple_of(sp * TOK, TOK), TOK)
    for ten in range(3):
        local[ten].wait()

        def send_qkv(i, _, ten=ten):
            d = mod(SP_MULT * i, 16)
            t = mod(z + sign * (d // 4) + 4, 4) * 4 + mod(x + sign * mod(d, 4) + 4, 4)
            remote(
                qkv_s.at[ten, :, pl.ds(pl.multiple_of(t * 128, 128), 128)],
                qkv_r.at[ten, my_rows, :],
                qkv_send.at[ten],
                qkv_recv.at[ten],
                (t, dp),
            ).start()
            return 0

        lax.fori_loop(1, 16, send_qkv, 0)
        if ten == 0:
            local[3].wait()
            for s, step in enumerate((1, 3)):
                for h in range(2):
                    remote(
                        wsrc.at[pl.ds(1024 * h, 1024)],
                        wr.at[:, pl.ds(pl.multiple_of(dp * 256, 256), 256)],
                        w_send.at[2 * s + h],
                        w_near.at[s],
                        (sp, mod(y + step, 4) * 2 + h),
                    ).start()
            remote(
                wsrc.at[pl.ds(pl.multiple_of((1 - c) * 1024, 1024), 1024)],
                wr.at[:, pl.ds(pl.multiple_of(dp * 256, 256), 256)],
                w_send.at[4],
                w_part,
                (sp, y * 2 + 1 - c),
            ).start()
        qkv_r[ten, my_rows, :] = qkv_s[ten, :, pl.ds(pl.multiple_of(sp * 128, 128), 128)]
    for k in range(1, 8):
        pl.semaphore_signal(ready, inc=1, device_id=(sp, mod(dp + k, 8)), device_id_type=MESH)
    experts = []
    for n, (src, dst) in enumerate(((eg_h, wg), (eu_h, wu), (ed_h, wd))):
        copy = pltpu.make_async_copy(src, dst, loc_sem.at[6 + n])
        copy.start()
        experts.append(copy)

    def expert_of(i):
        d = (MULT * i) & 127
        dz, dx, dy, dc = d & 3, (d >> 2) & 3, (d >> 4) & 3, d >> 6
        ts = ((z + sign * dz + 4) & 3) * 4 + ((x + sign * dx + 4) & 3)
        td = ((y + sign * dy + 4) & 3) * 2 + ((c + dc) & 1)
        return ts * 8 + td

    routes = routes_ref[...]
    r_col = [jnp.broadcast_to(routes[:, k : k + 1].astype(F32), (TOK, 128)) for k in range(2)]
    r_row = [m.T for m in r_col]
    lane = iota((TOK, 128), 1)
    sub = iota((TOK, 128), 0)
    hit_c = [(m == lane.astype(F32)).astype(F32) for m in r_col]
    hit_r = [(m == sub.astype(F32)).astype(F32) for m in r_row]
    lower = (lane < sub).astype(F32).astype(BF16)
    upper = (sub < lane).astype(F32).astype(BF16)
    before_c = dot(lower, (hit_c[0] + hit_c[1]).astype(BF16))
    before_r = dot((hit_r[0] + hit_r[1]).astype(BF16), upper)
    slot_c = [
        4.0 * r_col[k][:, :1] + jnp.sum(before_c * hit_c[k], axis=1, keepdims=True) for k in range(2)
    ]
    slot_r = [
        4.0 * r_row[k][:1, :] + jnp.sum(before_r * hit_r[k], axis=0, keepdims=True) for k in range(2)
    ]
    row = iota((1024, 128), 0)
    row_slot = (4 * expert_of(row >> 3) + (row & 3)).astype(F32)
    row_half = (row >> 2) & 1
    chosen = (row_slot == slot_r[0]) | (row_slot == slot_r[1])
    for g in range(2):
        disp[:, g * 128 : (g + 1) * 128] = jnp.where(chosen & (row_half == g), 1.0, 0.0).astype(BF16)
    col = iota((TOK, 1024), 1)
    col_slot = (4 * expert_of(col >> 3) + (col & 3)).astype(F32)
    col_half = (col >> 2) & 1
    for k in range(2):
        for g in range(2):
            at = (2 * k + g) * 128
            pick[at : at + 128, :] = jnp.where(
                (col_slot == slot_c[k]) & (col_half == g), 1.0, 0.0
            ).astype(BF16)
    shares = ish_ref[...]
    group = jnp.broadcast_to(gw_ref[...], (TOK, 128)).T[:, :1]
    share_sum = shares[:, 0:1] + shares[:, 1:2]
    for k in range(2):
        wts[k] = jnp.broadcast_to(group * shares[:, k : k + 1] / share_sum, (TOK, 128))
    p_o, p_i = iota((256, 256), 0), iota((256, 256), 1)
    perm[0] = jnp.where(
        p_i == 8 * ((p_o >> 2) & 31) + 4 * (p_o >> 7) + (p_o & 3), 1.0, 0.0
    ).astype(BF16)
    perm[1] = jnp.where(
        p_o == 8 * ((p_i >> 2) & 31) + 4 * (p_i >> 7) + (p_i & 3), 1.0, 0.0
    ).astype(BF16)

    def normed_heads(ten, at, size, gain_ref):
        rows = qkv_r[ten, at : at + size, :].astype(F32)
        square = rows * rows
        first = iota((size, 128), 1) < HD
        sum0 = jnp.sum(jnp.where(first, square, 0.0), axis=1, keepdims=True)
        sum1 = jnp.sum(jnp.where(first, 0.0, square), axis=1, keepdims=True)
        factor = jnp.where(
            first, lax.rsqrt(sum0 * (1.0 / HD) + EPS), lax.rsqrt(sum1 * (1.0 / HD) + EPS)
        )
        return (rows * factor * gain_ref[...]).astype(BF16).astype(F32)

    drain(qkv_r.at[0, pl.ds(0, 15 * TOK)], qkv_recv.at[0])
    step = 512
    for at in range(0, SEQ, step):
        turned = normed_heads(0, at, step, kg_ref).T
        sub = iota((128, step), 0)
        for h in range(2):
            bias = fc_ref[h : h + 1, at : at + step]
            high = bias.astype(BF16).astype(F32)
            middle = (bias - high).astype(BF16).astype(F32)
            low = bias - high - middle
            base = 64 * (1 - h)
            extra = jnp.where(
                sub == base, high, jnp.where(sub == base + 1, middle, jnp.where(sub == base + 2, low, 0.0))
            )
            mine = (sub < HD) if h == 0 else (sub >= HD)
            kt[h, :, at : at + step] = jnp.where(mine, turned, extra).astype(BF16)
    drain(qkv_r.at[1, pl.ds(0, 15 * TOK)], qkv_recv.at[1])
    for at in range(0, SEQ, step):
        scaled = normed_heads(1, at, step, qg_ref) * (HD**-0.5)
        lane = iota((step, 128), 1)
        for h in range(2):
            base = 64 * (1 - h)
            mine = (lane < HD) if h == 0 else (lane >= HD)
            extra = jnp.where((lane >= base) & (lane < base + 3), -1.0, 0.0)
            qh[h, at : at + step, :] = jnp.where(mine, scaled, extra).astype(BF16)
    drain(qkv_r.at[2, pl.ds(0, 15 * TOK)], qkv_recv.at[2])

    half = sp // 8
    a_cols = pl.ds(pl.multiple_of(mod(sp, 8) * 128, 128), 128)
    a_rows = pl.ds(pl.multiple_of(c * TOK, TOK), TOK)

    def return_block(t):
        own = jnp.logical_and(sp == t, half == c)

        @pl.when(own)
        def _():
            ar[a_rows, a_cols] = ao[t * TOK : (t + 1) * TOK, :]

        @pl.when(jnp.logical_not(own))
        def _():
            remote(
                ao.at[pl.ds(t * TOK, TOK)], ar.at[a_rows, a_cols], a_send, a_recv, (t, y * 2 + half)
            ).start()

    blocks = SEQ // QB
    tri = iota((QB, QB), 1) <= iota((QB, QB), 0)
    first = iota((QB, 128), 1) < HD
    pending = None
    for n, i in enumerate(reversed(range(blocks))):
        at, keys = i * QB, (i + 1) * QB
        results = []
        for h in range(2):
            query = qh[h, at:keys, :]
            diag = jnp.where(tri, dot(query, kt[h, :, at:keys]), -jnp.inf)
            highest = jnp.max(diag, axis=1, keepdims=True)
            if at:
                past = dot(query, kt[h, :, :at])
                highest = jnp.maximum(highest, jnp.max(past, axis=1, keepdims=True))
            diag = jnp.exp(diag - highest)
            total = jnp.sum(diag, axis=1, keepdims=True)
            result = dot(diag.astype(BF16), qkv_r[2, at:keys, :])
            if at:
                past = jnp.exp(past - highest)
                total = total + jnp.sum(past, axis=1, keepdims=True)
                result = result + dot(past.astype(BF16), qkv_r[2, :at, :])
            results.append(result / total)
        ao[at:keys, :] = jnp.where(first, results[0], results[1]).astype(BF16)
        if pending is not None:
            return_block(2 * pending)
            return_block(2 * pending + 1)
        pending = i
        if n == 3:
            for s, (near, onward) in enumerate(((3, 1), (1, 3))):
                drain(wr.at[:, pl.ds(0, 512)], w_near.at[s])
                part = wr.at[pl.ds(512 * s, 512), pl.ds(pl.multiple_of(mod(y + near, 4) * 512, 512), 512)]
                remote(part, part, w_send.at[5 + s], w_far, (sp, mod(y + onward, 4) * 2 + c)).start()
    return_block(0)
    return_block(1)

    local[4].wait()
    local[5].wait()
    drain(wr.at[:, pl.ds(0, 256)], w_part)
    drain(wr.at[:, pl.ds(0, 512)], w_far)
    own_in = half == c

    @pl.when(own_in)
    def _():
        drain(ao.at[pl.ds(0, 15 * TOK)], a_recv)
        drain(ao.at[pl.ds(0, 15 * TOK)], a_send)

    @pl.when(jnp.logical_not(own_in))
    def _():
        drain(ao.at[pl.ds(0, 16 * TOK)], a_recv)
        drain(ao.at[pl.ds(0, 16 * TOK)], a_send)

    other = ar[pl.ds(pl.multiple_of((1 - c) * TOK, TOK), TOK), :]
    for n in range(4):
        cols = pl.ds(512 * n, 512)
        psend[n] = dot(other, wr[:, cols])
        remote(psend.at[n], precv.at[n], p_send, p_recv, (sp, y * 2 + 1 - c)).start()
    mine = ar[a_rows, :]
    parts = [dot(mine, wr[:, 512 * n : 512 * n + 512]) for n in range(4)]
    drain(precv, p_recv)
    mids = []
    square = None
    for n in range(4):
        cols = slice(512 * n, 512 * n + 512)
        mid = (resid_s[:, cols].astype(F32) + (parts[n] + precv[n])).astype(BF16)
        resid_s[:, cols] = mid
        mid = mid.astype(F32)
        mids.append(mid)
        term = jnp.sum(mid * mid, axis=1, keepdims=True)
        square = term if square is None else square + term
    factor = lax.rsqrt(square * (1.0 / D) + EPS)
    normed = [
        (mids[n] * factor * ng_ref[:, 512 * n : 512 * n + 512]).astype(BF16) for n in range(4)
    ]
    halves = [jnp.concatenate(normed[2 * g : 2 * g + 2], axis=1) for g in range(2)]
    stacked = jnp.concatenate(halves, axis=0)
    for b in range(4):
        send[b * 32 : (b + 1) * 32] = (
            dot(disp[b * 256 : (b + 1) * 256, :], stacked).astype(BF16).reshape(32, 8, 1024)
        )

    pl.semaphore_wait(ready, 7)

    def partner(i, way):
        d = mod(MULT * i, 128)
        dz, dx, dy, dc = mod(d, 4), mod(d // 4, 4), mod(d // 16, 4), d // 64
        ts = mod(z + way * dz + 4, 4) * 4 + mod(x + way * dx + 4, 4)
        td = mod(y + way * dy + 4, 4) * 2 + mod(c + dc, 2)
        return ts, td

    def send_rows(i, _):
        remote(send.at[i], recv.at[i], d_send, d_recv.at[i // 32], partner(i, sign)).start()
        return 0

    lax.fori_loop(1, 128, send_rows, 0)
    recv[0] = send[0]
    for copy in experts:
        copy.wait()

    def wait_block(ref, sem, b):
        @pl.when(b == 0)
        def _():
            drain(ref.at[pl.ds(0, 31)], sem.at[b])

        @pl.when(b > 0)
        def _():
            drain(ref.at[pl.ds(0, 32)], sem.at[b])

    def run_expert(b, _):
        wait_block(recv, d_recv, b)
        at = pl.multiple_of(b * 32, 32)
        rows = recv[pl.ds(at, 32)].reshape(256, 1024)
        rows = dot(perm[0], rows).astype(BF16)
        gate = dot(rows[:128], wg[:1024, :]) + dot(rows[128:], wg[1024:, :])
        up = dot(rows[:128], wu[:1024, :]) + dot(rows[128:], wu[1024:, :])
        hidden = (gate / (1.0 + jnp.exp(-gate)) * up).astype(BF16)
        result = [dot(hidden, wd[:, g * 1024 : (g + 1) * 1024]).astype(BF16) for g in range(2)]
        back = dot(perm[1], jnp.concatenate(result, axis=0)).astype(BF16)
        ysend[pl.ds(at, 32)] = back.reshape(32, 8, 1024)

        def send_back(i, _):
            d = mod(MULT * i, 128)
            src_sign = sign * (1 - 2 * (d // 64))
            remote(ysend.at[i], ret.at[i], r_send, r_recv.at[b], partner(i, -src_sign)).start()
            return 0

        lax.fori_loop(jnp.where(b == 0, 1, b * 32), b * 32 + 32, send_back, 0)

        @pl.when(b == 0)
        def _():
            ret[0] = ysend[0]

        return 0

    lax.fori_loop(0, 4, run_expert, 0)
    acc[...] = jnp.zeros_like(acc)

    def collect(b, _):
        wait_block(ret, r_recv, b)
        rows = ret[pl.ds(pl.multiple_of(b * 32, 32), 32)].reshape(256, 1024)
        acc[...] += dot(pick[:, pl.ds(pl.multiple_of(b * 256, 256), 256)], rows)
        return 0

    lax.fori_loop(0, 4, collect, 0)
    for g in range(2):
        cols = slice(1024 * g, 1024 * g + 1024)
        mixed = wts[0][:, :1] * acc[g * 128 : g * 128 + 128, :]
        mixed = mixed + wts[1][:, :1] * acc[(2 + g) * 128 : (3 + g) * 128, :]
        out_ref[:, cols] = (resid_s[:, cols].astype(F32) + mixed).astype(BF16)

    for ten in range(3):
        drain(qkv_r.at[ten, pl.ds(0, 15 * TOK)], qkv_send.at[ten])
    for n in range(5):
        drain(wr.at[:, pl.ds(0, 256)], w_send.at[n])
    for n in range(5, 7):
        drain(wr.at[:, pl.ds(0, 256)], w_send.at[n])
    drain(precv, p_send)
    drain(recv.at[pl.ds(0, 127)], d_send)
    drain(recv.at[pl.ds(0, 127)], r_send)


def shards(
    resid,
    queries,
    keys,
    values,
    forget_cache,
    query_gain,
    key_gain,
    out_weight,
    norm_gain,
    routes,
    group_weight,
    inner_share,
    expert_gate,
    expert_up,
    expert_down,
):
    any_spec = pl.BlockSpec(memory_space=pl.ANY)
    vmem_spec = pl.BlockSpec(memory_space=pltpu.VMEM)
    vm = pltpu.VMEM
    dma = pltpu.SemaphoreType.DMA
    out = pl.pallas_call(
        kernel,
        out_shape=jax.ShapeDtypeStruct((TOK, D), BF16),
        in_specs=[any_spec] * 8 + [vmem_spec] * 7,
        out_specs=vmem_spec,
        scratch_shapes=[
            vm((3, TOK, D), BF16),
            vm((3, SEQ, 128), BF16),
            vm((2, SEQ, 128), BF16),
            vm((2, 128, SEQ), BF16),
            vm((SEQ, 128), BF16),
            vm((2 * TOK, 1024), BF16),
            vm((D, 256), BF16),
            vm((1024, D), BF16),
            vm((4, TOK, 512), F32),
            vm((4, TOK, 512), F32),
            vm((TOK, D), BF16),
            vm((1024, 256), BF16),
            vm((512, 1024), BF16),
            vm((2, 256, 256), BF16),
            vm((D, FF), BF16),
            vm((D, FF), BF16),
            vm((FF, D), BF16),
            vm((128, 8, 1024), BF16),
            vm((128, 8, 1024), BF16),
            vm((128, 8, 1024), BF16),
            vm((128, 8, 1024), BF16),
            vm((512, 1024), F32),
            vm((2, TOK, 128), F32),
            dma((9,)),
            dma((3,)),
            dma((3,)),
            dma((7,)),
            dma((2,)),
            dma,
            dma,
            dma,
            dma,
            dma,
            dma,
            dma,
            dma((4,)),
            dma,
            dma((4,)),
            pltpu.SemaphoreType.REGULAR,
        ],
        compiler_params=pltpu.CompilerParams(
            collective_id=0, has_side_effects=True, vmem_limit_bytes=62 * 2**20
        ),
        name="layer",
    )(
        queries[0],
        keys[0],
        values[0],
        resid[0],
        out_weight,
        expert_gate[0],
        expert_up[0],
        expert_down[0],
        forget_cache[0],
        jnp.tile(query_gain, 2).reshape(1, 128),
        jnp.tile(key_gain, 2).reshape(1, 128),
        norm_gain.reshape(1, D),
        routes[0],
        group_weight,
        inner_share[0],
    )
    return out[None]


def solution(mesh):
    return jax.shard_map(
        shards,
        mesh=mesh,
        in_specs=(
            P("dp", "sp", None),
            P("dp", "sp", None),
            P("dp", "sp", None),
            P("dp", "sp", None),
            P("dp", "sp", None),
            P(),
            P(),
            P(None, "dp"),
            P(),
            P("dp", "sp", None),
            P("dp", "sp"),
            P("dp", "sp", None),
            P(("sp", "dp"), None, None),
            P(("sp", "dp"), None, None),
            P(("sp", "dp"), None, None),
        ),
        out_specs=P("dp", "sp", None),
        check_vma=False,
    )
```

time: 255 us -> 110 us (0.43)
  Pallas kernels: 0 us -> 103 us
  waiting for transfers between devices: 70.2 us -> 0 us
  matrix products: 62.7 us -> 0 us
  blocking collectives: 37.1 us -> 0 us
  local copies, waits for them, and re-layouts: 28.2 us -> 7.25 us
  other arithmetic: 20.9 us -> 0 us
  starting transfers between devices: 18.6 us -> 0 us
  between operations: 13.8 us -> 0.01 us
  loops' own time: 2.88 us -> 0 us
    pallas_call x0 -> x1, Pallas kernels: none -> 103 us  [shards(): pl.pallas_call(kernel, out_shape=jax.ShapeDtypeStruct((TOK, D), BF16), in...]
    all_to_all x3 -> x0, waiting for transfers between devices: 69.4 us -> none  [the longest x1 30.3 us: side_by_side(): lax.all_to_all(both, axis, split_axis=split_dim, concat_axis=concat_dim,...]
    dot_general x10 -> x0, matrix products: 43.8 us -> none  [the longest x4 19.9 us: attend(): jnp.einsum('hqk,khd->qhd', probs, value_rows, preferred_element_type=jnp....]
    all_to_all x1 -> x0, blocking collectives: 37.1 us -> none  [shards(): lax.all_to_all(send.reshape(experts, capacity, width), ('sp', 'dp'), spli...]
    sub x4 -> x0, matrix products: 18.8 us -> none  [attend(): expd = jnp.exp(scores - highest)]
    all_to_all x3 -> x0, starting transfers between devices: 18.5 us -> none  [the longest x1 8.42 us: side_by_side(): lax.all_to_all(both, axis, split_axis=split_dim, concat_axis=concat_dim,...]
    reshape x6 -> x0, local copies, waits for them, and re-layouts: 12.4 us -> none  [the longest x1 4.13 us: shards(): result.reshape(arrived.shape)]
    unnamed x1 -> x0, other arithmetic: 11.8 us -> none
  transfers between devices with their start and end apart: 4 -> 0, of which waited for: 3 -> 0; matrix products, arithmetic and copies ran while one was open for 30% -> 0% of each run, Pallas kernels for 0% -> 0%
where the time goes in v1:
time: 110 us
  Pallas kernels  103 us (94%)
  local copies, waits for them, and re-layouts  7.25 us (7%)
    pallas_call x1, Pallas kernels, shards(): pl.pallas_call(kernel, out_shape=jax.ShapeDtypeStruct((TOK, D), BF16), in...  103 us
    unnamed x3, local copies, waits for them, and re-layouts  4.7 us

profile of v1, /device:TPU:1, one launch (start us, length us, event | category | flops | bytes accessed | tf_op | source)
XLA Modules:
  0.0 109.9 jit_solution(3001691825139901480)
XLA Ops:
  0.0 0.7 tile.4
  0.7 0.6 reshape_tile.6.qg_ref
  1.2 0.7 tile.5
  1.9 0.7 reshape_tile.7.kg_ref
  2.6 1.4 %copy.16 = s32[1,128,2]{2,1,0:T(8,128)} copy(s32[1,128,2]{1,2,0:T(2,128)} %param.24) | data formatting | bytes 2048 | tf_op args[9]
  4.0 1.4 %copy.17 = f32[1,128,2]{2,1,0:T(8,128)} copy(f32[1,128,2]{1,2,0:T(2,128)} %param.26) | data formatting | bytes 2048 | tf_op args[11]
  5.4 102.6 %layer.1 = bf16[128,2048]{1,0:T(8,128)(2,1)} custom-call(bf16[128,2048]{1,0:T(8,128)(2,1)} %bitcast.16, bf16[128,2048]{1,0:T(8,128)(2,1)} %bitcast.17, bf16[128,2048]{1,0:T(8,128)(2,1)} %bitcast.18, bf16[128,2048]{1,0:T(8,128)(2,1)} %bitcast.19, bf16[2048,256]{1,0:T(8,128)(2,1)} %ow_h.1, bf16[2048,1024]{1,0:T(8,128)(2,1)} %bitcast.12, ...), custom_call_target="tpu_custom_call" | custom-call | tf_op jit(solution)/shard_map/layer/pallas_call | solution.py:462
  108.0 1.9 %copy.19 = bf16[1,128,2048]{2,1,0:T(8,128)(2,1)} copy(bf16[1,128,2048]{2,1,0:T(8,128)(2,1)} %bitcast.15) | data formatting | bytes 1048576

commit v2 on v1

--- a/solution.py
+++ b/solution.py
@@ -60,7 +60,8 @@
     kt,
     ao,
     ar,
-    wsrc,
+    probs,
+    scale,
     wr,
     psend,
     precv,
@@ -84,6 +85,7 @@
     w_near,
     w_far,
     w_part,
+    w_swap,
     a_send,
     a_recv,
     p_send,
@@ -99,6 +101,7 @@
     z, x = sp // 4, mod(sp, 4)
     y, c = dp // 2, mod(dp, 2)
     sign = 1 - 2 * c
+    parity = mod(z + x, 2)
 
     local = []
     for n, (src, dst) in enumerate(
@@ -106,7 +109,6 @@
             (k_h, qkv_s.at[0]),
             (q_h, qkv_s.at[1]),
             (v_h, qkv_s.at[2]),
-            (ow_h, wsrc),
             (ow_h.at[pl.ds(pl.multiple_of(c * 1024, 1024), 1024)],
              wr.at[:, pl.ds(pl.multiple_of(dp * 256, 256), 256)]),
             (resid_h, resid_s),
@@ -127,6 +129,19 @@
             src_ref=src, dst_ref=dst, send_sem=ssem, recv_sem=rsem, device_id=dev, device_id_type=MESH
         )
 
+    my_cols = pl.ds(pl.multiple_of(dp * 256, 256), 256)
+
+    def send_near(part, ssem, rsem):
+        for step in (1, 3):
+            for h in range(2):
+                remote(
+                    ow_h.at[pl.ds(pl.multiple_of(1024 * h + 512 * part, 512), 512)],
+                    wr.at[pl.ds(pl.multiple_of(512 * part, 512), 512), my_cols],
+                    ssem,
+                    rsem,
+                    (sp, mod(y + step, 4) * 2 + h),
+                ).start()
+
     my_rows = pl.ds(pl.multiple_of(sp * TOK, TOK), TOK)
     for ten in range(3):
         local[ten].wait()
@@ -145,20 +160,11 @@
 
         lax.fori_loop(1, 16, send_qkv, 0)
         if ten == 0:
-            local[3].wait()
-            for s, step in enumerate((1, 3)):
-                for h in range(2):
-                    remote(
-                        wsrc.at[pl.ds(1024 * h, 1024)],
-                        wr.at[:, pl.ds(pl.multiple_of(dp * 256, 256), 256)],
-                        w_send.at[2 * s + h],
-                        w_near.at[s],
-                        (sp, mod(y + step, 4) * 2 + h),
-                    ).start()
+            send_near(parity, w_send.at[0], w_near.at[0])
             remote(
-                wsrc.at[pl.ds(pl.multiple_of((1 - c) * 1024, 1024), 1024)],
-                wr.at[:, pl.ds(pl.multiple_of(dp * 256, 256), 256)],
-                w_send.at[4],
+                ow_h.at[pl.ds(pl.multiple_of((1 - c) * 1024, 1024), 1024)],
+                wr.at[:, my_cols],
+                w_send.at[1],
                 w_part,
                 (sp, y * 2 + 1 - c),
             ).start()
@@ -167,7 +173,7 @@
         pl.semaphore_signal(ready, inc=1, device_id=(sp, mod(dp + k, 8)), device_id_type=MESH)
     experts = []
     for n, (src, dst) in enumerate(((eg_h, wg), (eu_h, wu), (ed_h, wd))):
-        copy = pltpu.make_async_copy(src, dst, loc_sem.at[6 + n])
+        copy = pltpu.make_async_copy(src, dst, loc_sem.at[5 + n])
         copy.start()
         experts.append(copy)
 
@@ -178,9 +184,10 @@
         td = ((y + sign * dy + 4) & 3) * 2 + ((c + dc) & 1)
         return ts * 8 + td
 
-    routes = routes_ref[...]
-    r_col = [jnp.broadcast_to(routes[:, k : k + 1].astype(F32), (TOK, 128)) for k in range(2)]
-    r_row = [m.T for m in r_col]
+    r_row = [
+        jnp.broadcast_to(routes_ref[k : k + 1, :].astype(F32), (128, TOK)) for k in range(2)
+    ]
+    r_col = [m.T for m in r_row]
     lane = iota((TOK, 128), 1)
     sub = iota((TOK, 128), 0)
     hit_c = [(m == lane.astype(F32)).astype(F32) for m in r_col]
@@ -210,11 +217,10 @@
             pick[at : at + 128, :] = jnp.where(
                 (col_slot == slot_c[k]) & (col_half == g), 1.0, 0.0
             ).astype(BF16)
-    shares = ish_ref[...]
-    group = jnp.broadcast_to(gw_ref[...], (TOK, 128)).T[:, :1]
-    share_sum = shares[:, 0:1] + shares[:, 1:2]
+    share_sum = ish_ref[0:1, :] + ish_ref[1:2, :]
     for k in range(2):
-        wts[k] = jnp.broadcast_to(group * shares[:, k : k + 1] / share_sum, (TOK, 128))
+        weight = gw_ref[...] * ish_ref[k : k + 1, :] / share_sum
+        wts[k] = jnp.broadcast_to(weight, (128, TOK)).T
     p_o, p_i = iota((256, 256), 0), iota((256, 256), 1)
     perm[0] = jnp.where(
         p_i == 8 * ((p_o >> 2) & 31) + 4 * (p_o >> 7) + (p_o & 3), 1.0, 0.0
@@ -232,7 +238,8 @@
         factor = jnp.where(
             first, lax.rsqrt(sum0 * (1.0 / HD) + EPS), lax.rsqrt(sum1 * (1.0 / HD) + EPS)
         )
-        return (rows * factor * gain_ref[...]).astype(BF16).astype(F32)
+        gain = jnp.concatenate([gain_ref[...]] * 2, axis=1)
+        return (rows * factor * gain).astype(BF16).astype(F32)
 
     drain(qkv_r.at[0, pl.ds(0, 15 * TOK)], qkv_recv.at[0])
     step = 512
@@ -259,32 +266,40 @@
             mine = (lane < HD) if h == 0 else (lane >= HD)
             extra = jnp.where((lane >= base) & (lane < base + 3), -1.0, 0.0)
             qh[h, at : at + step, :] = jnp.where(mine, scaled, extra).astype(BF16)
-    drain(qkv_r.at[2, pl.ds(0, 15 * TOK)], qkv_recv.at[2])
+
+    drain(wr.at[pl.ds(0, 512), pl.ds(0, 1024)], w_near.at[0])
+    for s, (near, onward) in enumerate(((3, 1), (1, 3))):
+        part = wr.at[
+            pl.ds(pl.multiple_of(512 * parity + 256 * s, 256), 256),
+            pl.ds(pl.multiple_of(mod(y + near, 4) * 512, 512), 512),
+        ]
+        remote(part, part, w_send.at[2], w_far, (sp, mod(y + onward, 4) * 2 + c)).start()
+    send_near(1 - parity, w_send.at[4], w_near.at[1])
 
     half = sp // 8
     a_cols = pl.ds(pl.multiple_of(mod(sp, 8) * 128, 128), 128)
     a_rows = pl.ds(pl.multiple_of(c * TOK, TOK), TOK)
 
-    def return_block(t):
-        own = jnp.logical_and(sp == t, half == c)
-
-        @pl.when(own)
-        def _():
-            ar[a_rows, a_cols] = ao[t * TOK : (t + 1) * TOK, :]
-
-        @pl.when(jnp.logical_not(own))
-        def _():
-            remote(
-                ao.at[pl.ds(t * TOK, TOK)], ar.at[a_rows, a_cols], a_send, a_recv, (t, y * 2 + half)
-            ).start()
+    def return_block(i):
+        for t in (2 * i, 2 * i + 1):
+            own = jnp.logical_and(sp == t, half == c)
+            rows = pl.ds(pl.multiple_of(t * TOK, TOK), TOK)
+
+            @pl.when(own)
+            def _(rows=rows):
+                ar[a_rows, a_cols] = ao[rows, :]
+
+            @pl.when(jnp.logical_not(own))
+            def _(rows=rows, t=t):
+                remote(ao.at[rows], ar.at[a_rows, a_cols], a_send, a_recv, (t, y * 2 + half)).start()
 
     blocks = SEQ // QB
     tri = iota((QB, QB), 1) <= iota((QB, QB), 0)
     first = iota((QB, 128), 1) < HD
-    pending = None
-    for n, i in enumerate(reversed(range(blocks))):
+
+    def weigh(i):
         at, keys = i * QB, (i + 1) * QB
-        results = []
+        inverse = []
         for h in range(2):
             query = qh[h, at:keys, :]
             diag = jnp.where(tri, dot(query, kt[h, :, at:keys]), -jnp.inf)
@@ -294,29 +309,58 @@
                 highest = jnp.maximum(highest, jnp.max(past, axis=1, keepdims=True))
             diag = jnp.exp(diag - highest)
             total = jnp.sum(diag, axis=1, keepdims=True)
-            result = dot(diag.astype(BF16), qkv_r[2, at:keys, :])
+            tile = i * (i + 1) // 2
+            probs[h, tile + i] = diag.astype(BF16)
             if at:
                 past = jnp.exp(past - highest)
                 total = total + jnp.sum(past, axis=1, keepdims=True)
-                result = result + dot(past.astype(BF16), qkv_r[2, :at, :])
-            results.append(result / total)
-        ao[at:keys, :] = jnp.where(first, results[0], results[1]).astype(BF16)
-        if pending is not None:
-            return_block(2 * pending)
-            return_block(2 * pending + 1)
-        pending = i
-        if n == 3:
-            for s, (near, onward) in enumerate(((3, 1), (1, 3))):
-                drain(wr.at[:, pl.ds(0, 512)], w_near.at[s])
-                part = wr.at[pl.ds(512 * s, 512), pl.ds(pl.multiple_of(mod(y + near, 4) * 512, 512), 512)]
-                remote(part, part, w_send.at[5 + s], w_far, (sp, mod(y + onward, 4) * 2 + c)).start()
-    return_block(0)
-    return_block(1)
-
+                for j in range(i):
+                    probs[h, tile + j] = past[:, j * QB : (j + 1) * QB].astype(BF16)
+            inverse.append(1.0 / total)
+        scale[at:keys, :] = jnp.where(first, inverse[0], inverse[1])
+
+    def combine(i):
+        at, keys = i * QB, (i + 1) * QB
+        results = []
+        for h in range(2):
+            result = None
+            for j in range(i + 1):
+                term = dot(probs[h, i * (i + 1) // 2 + j], qkv_r[2, j * QB : (j + 1) * QB, :])
+                result = term if result is None else result + term
+            results.append(result)
+        ao[at:keys, :] = (jnp.where(first, results[0], results[1]) * scale[at:keys, :]).astype(BF16)
+
+    def block_of(n):
+        m = mod(n + sp // 2, blocks)
+        odd = mod(m, 2)
+        return (1 - odd) * (blocks - 1 - m // 2) + odd * (m // 2)
+
+    for i in range(blocks):
+        weigh(i)
+    drain(qkv_r.at[2, pl.ds(0, 15 * TOK)], qkv_recv.at[2])
+
+    def one_block(n, _):
+        for i in range(blocks):
+            pl.when(block_of(n) == i)(functools.partial(combine, i))
+        return_block(block_of(n))
+        return 0
+
+    lax.fori_loop(0, blocks, one_block, 0)
+    drain(wr.at[pl.ds(0, 512), pl.ds(0, 512)], w_far)
+    for q, t in enumerate((
+        z * 4 + mod(x + 1, 4), z * 4 + mod(x + 3, 4), mod(z + 1, 4) * 4 + x, mod(z + 3, 4) * 4 + x
+    )):
+        part = wr.at[
+            pl.ds(pl.multiple_of(512 * parity + 128 * q, 128), 128),
+            pl.ds(pl.multiple_of(mod(y + 2, 4) * 512, 512), 512),
+        ]
+        remote(part, part, w_send.at[3], w_swap, (t, dp)).start()
+
+    local[3].wait()
     local[4].wait()
-    local[5].wait()
     drain(wr.at[:, pl.ds(0, 256)], w_part)
-    drain(wr.at[:, pl.ds(0, 512)], w_far)
+    drain(wr.at[pl.ds(0, 512), pl.ds(0, 1024)], w_near.at[1])
+    drain(wr.at[pl.ds(0, 512), pl.ds(0, 512)], w_swap)
     own_in = half == c
 
     @pl.when(own_in)
@@ -429,10 +473,11 @@
 
     for ten in range(3):
         drain(qkv_r.at[ten, pl.ds(0, 15 * TOK)], qkv_send.at[ten])
-    for n in range(5):
-        drain(wr.at[:, pl.ds(0, 256)], w_send.at[n])
-    for n in range(5, 7):
-        drain(wr.at[:, pl.ds(0, 256)], w_send.at[n])
+    drain(wr.at[pl.ds(0, 512), pl.ds(0, 1024)], w_send.at[0])
+    drain(wr.at[:, pl.ds(0, 256)], w_send.at[1])
+    drain(wr.at[pl.ds(0, 512), pl.ds(0, 512)], w_send.at[2])
+    drain(wr.at[pl.ds(0, 512), pl.ds(0, 512)], w_send.at[3])
+    drain(wr.at[pl.ds(0, 512), pl.ds(0, 1024)], w_send.at[4])
     drain(precv, p_send)
     drain(recv.at[pl.ds(0, 127)], d_send)
     drain(recv.at[pl.ds(0, 127)], r_send)
@@ -455,14 +500,14 @@
     expert_up,
     expert_down,
 ):
-    any_spec = pl.BlockSpec(memory_space=pl.ANY)
+    hbm_spec = pl.BlockSpec(memory_space=pltpu.HBM)
     vmem_spec = pl.BlockSpec(memory_space=pltpu.VMEM)
     vm = pltpu.VMEM
     dma = pltpu.SemaphoreType.DMA
     out = pl.pallas_call(
         kernel,
         out_shape=jax.ShapeDtypeStruct((TOK, D), BF16),
-        in_specs=[any_spec] * 8 + [vmem_spec] * 7,
+        in_specs=[hbm_spec] * 8 + [vmem_spec] * 7,
         out_specs=vmem_spec,
         scratch_shapes=[
             vm((3, TOK, D), BF16),
@@ -471,7 +516,8 @@
             vm((2, 128, SEQ), BF16),
             vm((SEQ, 128), BF16),
             vm((2 * TOK, 1024), BF16),
-            vm((D, 256), BF16),
+            vm((2, 36, QB, QB), BF16),
+            vm((SEQ, 128), F32),
             vm((1024, D), BF16),
             vm((4, TOK, 512), F32),
             vm((4, TOK, 512), F32),
@@ -491,8 +537,9 @@
             dma((9,)),
             dma((3,)),
             dma((3,)),
-            dma((7,)),
+            dma((5,)),
             dma((2,)),
+            dma,
             dma,
             dma,
             dma,
@@ -506,25 +553,30 @@
             pltpu.SemaphoreType.REGULAR,
         ],
         compiler_params=pltpu.CompilerParams(
-            collective_id=0, has_side_effects=True, vmem_limit_bytes=62 * 2**20
+            collective_id=0, has_side_effects=True, vmem_limit_bytes=53 * 2**20
         ),
         name="layer",
     )(
-        queries[0],
-        keys[0],
-        values[0],
-        resid[0],
-        out_weight,
-        expert_gate[0],
-        expert_up[0],
-        expert_down[0],
-        forget_cache[0],
-        jnp.tile(query_gain, 2).reshape(1, 128),
-        jnp.tile(key_gain, 2).reshape(1, 128),
-        norm_gain.reshape(1, D),
-        routes[0],
-        group_weight,
-        inner_share[0],
+        *[
+            pltpu.with_memory_space_constraint(a, pltpu.HBM)
+            for a in (
+                queries[0],
+                keys[0],
+                values[0],
+                resid[0],
+                out_weight,
+                expert_gate[0],
+                expert_up[0],
+                expert_down[0],
+                forget_cache[0],
+                query_gain.reshape(1, HD),
+                key_gain.reshape(1, HD),
+                norm_gain.reshape(1, D),
+                routes[0].T,
+                group_weight,
+                inner_share[0].T,
+            )
+        ]
     )
     return out[None]
 

time: 110 us -> 97.7 us (0.89)
  local copies, waits for them, and re-layouts: 7.25 us -> 0.8 us
  Pallas kernels: 103 us -> 96.8 us
    pallas_call x1, Pallas kernels: 103 us -> 96.8 us  [shards(): pl.pallas_call(kernel, out_shape=jax.ShapeDtypeStruct((TOK, D), BF16), in...]
    unnamed x3 -> x1, local copies, waits for them, and re-layouts: 4.7 us -> 0.8 us
    another operation x4 -> x0, local copies, waits for them, and re-layouts: 2.55 us -> none  [the longest x2 1.31 us: shards(): jnp.tile(key_gain, 2).reshape(1, 128)]
where the time goes in v2:
time: 97.7 us; the launch traced here: 97.6 us
  Pallas kernels  96.8 us (99%)
    pallas_call x1, Pallas kernels, shards(): pl.pallas_call(kernel, out_shape=jax.ShapeDtypeStruct((TOK, D), BF16), in...  96.8 us

profile of v2, /device:TPU:1, one launch (start us, length us, event | category | flops | bytes accessed | tf_op | source)
XLA Modules:
  0.0 97.6 jit_solution(9492595784053437094)
XLA Ops:
  0.0 96.8 %layer.1 = bf16[128,2048]{1,0:T(8,128)(2,1)S(1)} custom-call(bf16[128,2048]{1,0:T(8,128)(2,1)} %bitcast.22, bf16[128,2048]{1,0:T(8,128)(2,1)} %bitcast.23, bf16[128,2048]{1,0:T(8,128)(2,1)} %bitcast.24, bf16[128,2048]{1,0:T(8,128)(2,1)} %bitcast.25, bf16[2048,256]{1,0:T(8,128)(2,1)} %ow_h.1, bf16[2048,1024]{1,0:T(8,128)(2,1)} %bitcast.19, ...), custom_call_target="tpu_custom_call" | custom-call | tf_op jit(solution)/shard_map/layer/pallas_call | solution.py:507
  96.8 0.8 copy.17

commit v3 on v2

--- a/solution.py
+++ b/solution.py
@@ -17,7 +17,7 @@
 TOK = 128
 SEQ = 2048
 QB = 256
-MULT = 37
+MULT = 27
 SP_MULT = 7
 
 
@@ -46,6 +46,14 @@
     eg_h,
     eu_h,
     ed_h,
+    fc_h,
+    qg_h,
+    kg_h,
+    ng_h,
+    routes_h,
+    gw_h,
+    ish_h,
+    out_ref,
     fc_ref,
     qg_ref,
     kg_ref,
@@ -53,7 +61,6 @@
     routes_ref,
     gw_ref,
     ish_ref,
-    out_ref,
     qkv_s,
     qkv_r,
     qh,
@@ -85,7 +92,6 @@
     w_near,
     w_far,
     w_part,
-    w_swap,
     a_send,
     a_recv,
     p_send,
@@ -103,6 +109,11 @@
     sign = 1 - 2 * c
     parity = mod(z + x, 2)
 
+    barrier = pltpu.get_barrier_semaphore()
+    for k in range(1, 16):
+        pl.semaphore_signal(barrier, inc=1, device_id=(mod(sp + k, 16), dp), device_id_type=MESH)
+    for k in range(1, 8):
+        pl.semaphore_signal(barrier, inc=1, device_id=(sp, mod(dp + k, 8)), device_id_type=MESH)
     local = []
     for n, (src, dst) in enumerate(
         (
@@ -112,16 +123,18 @@
             (ow_h.at[pl.ds(pl.multiple_of(c * 1024, 1024), 1024)],
              wr.at[:, pl.ds(pl.multiple_of(dp * 256, 256), 256)]),
             (resid_h, resid_s),
+            (routes_h, routes_ref),
+            (gw_h, gw_ref),
+            (ish_h, ish_ref),
+            (fc_h, fc_ref),
+            (kg_h, kg_ref),
+            (qg_h, qg_ref),
+            (ng_h, ng_ref),
         )
     ):
         copy = pltpu.make_async_copy(src, dst, loc_sem.at[n])
         copy.start()
         local.append(copy)
-    barrier = pltpu.get_barrier_semaphore()
-    for k in range(1, 16):
-        pl.semaphore_signal(barrier, inc=1, device_id=(mod(sp + k, 16), dp), device_id_type=MESH)
-    for k in range(1, 8):
-        pl.semaphore_signal(barrier, inc=1, device_id=(sp, mod(dp + k, 8)), device_id_type=MESH)
     pl.semaphore_wait(barrier, 22)
 
     def remote(src, dst, ssem, rsem, dev):
@@ -131,12 +144,12 @@
 
     my_cols = pl.ds(pl.multiple_of(dp * 256, 256), 256)
 
-    def send_near(part, ssem, rsem):
+    def send_near(start, size, ssem, rsem):
         for step in (1, 3):
             for h in range(2):
                 remote(
-                    ow_h.at[pl.ds(pl.multiple_of(1024 * h + 512 * part, 512), 512)],
-                    wr.at[pl.ds(pl.multiple_of(512 * part, 512), 512), my_cols],
+                    ow_h.at[pl.ds(pl.multiple_of(1024 * h + start, 256), size)],
+                    wr.at[pl.ds(pl.multiple_of(start, 256), size), my_cols],
                     ssem,
                     rsem,
                     (sp, mod(y + step, 4) * 2 + h),
@@ -160,7 +173,8 @@
 
         lax.fori_loop(1, 16, send_qkv, 0)
         if ten == 0:
-            send_near(parity, w_send.at[0], w_near.at[0])
+            send_near(512 * parity, 512, w_send.at[0], w_near.at[0])
+            send_near(512 * (1 - parity), 256, w_send.at[4], w_near.at[1])
             remote(
                 ow_h.at[pl.ds(pl.multiple_of((1 - c) * 1024, 1024), 1024)],
                 wr.at[:, my_cols],
@@ -173,9 +187,12 @@
         pl.semaphore_signal(ready, inc=1, device_id=(sp, mod(dp + k, 8)), device_id_type=MESH)
     experts = []
     for n, (src, dst) in enumerate(((eg_h, wg), (eu_h, wu), (ed_h, wd))):
-        copy = pltpu.make_async_copy(src, dst, loc_sem.at[5 + n])
+        copy = pltpu.make_async_copy(src, dst, loc_sem.at[12 + n])
         copy.start()
         experts.append(copy)
+
+    for copy in local[5:]:
+        copy.wait()
 
     def expert_of(i):
         d = (MULT * i) & 127
@@ -268,13 +285,26 @@
             qh[h, at : at + step, :] = jnp.where(mine, scaled, extra).astype(BF16)
 
     drain(wr.at[pl.ds(0, 512), pl.ds(0, 1024)], w_near.at[0])
-    for s, (near, onward) in enumerate(((3, 1), (1, 3))):
-        part = wr.at[
-            pl.ds(pl.multiple_of(512 * parity + 256 * s, 256), 256),
-            pl.ds(pl.multiple_of(mod(y + near, 4) * 512, 512), 512),
-        ]
-        remote(part, part, w_send.at[2], w_far, (sp, mod(y + onward, 4) * 2 + c)).start()
-    send_near(1 - parity, w_send.at[4], w_near.at[1])
+    def relay(start, ssem, rsem):
+        for s, (near, onward) in enumerate(((3, 1), (1, 3))):
+            part = wr.at[
+                pl.ds(pl.multiple_of(start + 256 * s, 256), 256),
+                pl.ds(pl.multiple_of(mod(y + near, 4) * 512, 512), 512),
+            ]
+            remote(part, part, ssem, rsem, (sp, mod(y + onward, 4) * 2 + c)).start()
+
+    relay(512 * parity, w_send.at[2], w_far.at[0])
+    across = (
+        z * 4 + mod(x + 1, 4), z * 4 + mod(x + 3, 4), mod(z + 1, 4) * 4 + x, mod(z + 3, 4) * 4 + x
+    )
+
+    for step in (1, 3):
+        for q, t in enumerate(across):
+            part = wr.at[
+                pl.ds(pl.multiple_of(512 * parity + 256 + 64 * q, 64), 64),
+                pl.ds(pl.multiple_of(mod(y + step, 4) * 512, 512), 512),
+            ]
+            remote(part, part, w_send.at[5], w_near.at[2], (t, dp)).start()
 
     half = sp // 8
     a_cols = pl.ds(pl.multiple_of(mod(sp, 8) * 128, 128), 128)
@@ -338,6 +368,9 @@
     for i in range(blocks):
         weigh(i)
     drain(qkv_r.at[2, pl.ds(0, 15 * TOK)], qkv_recv.at[2])
+    drain(wr.at[pl.ds(0, 256), pl.ds(0, 1024)], w_near.at[1])
+    drain(wr.at[pl.ds(0, 256), pl.ds(0, 1024)], w_near.at[2])
+    relay(512 * (1 - parity), w_send.at[3], w_far.at[1])
 
     def one_block(n, _):
         for i in range(blocks):
@@ -346,21 +379,12 @@
         return 0
 
     lax.fori_loop(0, blocks, one_block, 0)
-    drain(wr.at[pl.ds(0, 512), pl.ds(0, 512)], w_far)
-    for q, t in enumerate((
-        z * 4 + mod(x + 1, 4), z * 4 + mod(x + 3, 4), mod(z + 1, 4) * 4 + x, mod(z + 3, 4) * 4 + x
-    )):
-        part = wr.at[
-            pl.ds(pl.multiple_of(512 * parity + 128 * q, 128), 128),
-            pl.ds(pl.multiple_of(mod(y + 2, 4) * 512, 512), 512),
-        ]
-        remote(part, part, w_send.at[3], w_swap, (t, dp)).start()
 
     local[3].wait()
     local[4].wait()
     drain(wr.at[:, pl.ds(0, 256)], w_part)
-    drain(wr.at[pl.ds(0, 512), pl.ds(0, 1024)], w_near.at[1])
-    drain(wr.at[pl.ds(0, 512), pl.ds(0, 512)], w_swap)
+    drain(wr.at[pl.ds(0, 512), pl.ds(0, 512)], w_far.at[0])
+    drain(wr.at[pl.ds(0, 512), pl.ds(0, 512)], w_far.at[1])
     own_in = half == c
 
     @pl.when(own_in)
@@ -397,11 +421,6 @@
     ]
     halves = [jnp.concatenate(normed[2 * g : 2 * g + 2], axis=1) for g in range(2)]
     stacked = jnp.concatenate(halves, axis=0)
-    for b in range(4):
-        send[b * 32 : (b + 1) * 32] = (
-            dot(disp[b * 256 : (b + 1) * 256, :], stacked).astype(BF16).reshape(32, 8, 1024)
-        )
-
     pl.semaphore_wait(ready, 7)
 
     def partner(i, way):
@@ -415,7 +434,11 @@
         remote(send.at[i], recv.at[i], d_send, d_recv.at[i // 32], partner(i, sign)).start()
         return 0
 
-    lax.fori_loop(1, 128, send_rows, 0)
+    for b in range(4):
+        send[b * 32 : (b + 1) * 32] = (
+            dot(disp[b * 256 : (b + 1) * 256, :], stacked).astype(BF16).reshape(32, 8, 1024)
+        )
+        lax.fori_loop(max(1, b * 32), b * 32 + 32, send_rows, 0)
     recv[0] = send[0]
     for copy in experts:
         copy.wait()
@@ -477,7 +500,8 @@
     drain(wr.at[:, pl.ds(0, 256)], w_send.at[1])
     drain(wr.at[pl.ds(0, 512), pl.ds(0, 512)], w_send.at[2])
     drain(wr.at[pl.ds(0, 512), pl.ds(0, 512)], w_send.at[3])
-    drain(wr.at[pl.ds(0, 512), pl.ds(0, 1024)], w_send.at[4])
+    drain(wr.at[pl.ds(0, 256), pl.ds(0, 1024)], w_send.at[4])
+    drain(wr.at[pl.ds(0, 256), pl.ds(0, 1024)], w_send.at[5])
     drain(precv, p_send)
     drain(recv.at[pl.ds(0, 127)], d_send)
     drain(recv.at[pl.ds(0, 127)], r_send)
@@ -507,9 +531,16 @@
     out = pl.pallas_call(
         kernel,
         out_shape=jax.ShapeDtypeStruct((TOK, D), BF16),
-        in_specs=[hbm_spec] * 8 + [vmem_spec] * 7,
+        in_specs=[hbm_spec] * 15,
         out_specs=vmem_spec,
         scratch_shapes=[
+            vm((2, SEQ), F32),
+            vm((1, HD), F32),
+            vm((1, HD), F32),
+            vm((1, D), F32),
+            vm((2, TOK), jnp.int32),
+            vm((1, TOK), F32),
+            vm((2, TOK), F32),
             vm((3, TOK, D), BF16),
             vm((3, SEQ, 128), BF16),
             vm((2, SEQ, 128), BF16),
@@ -534,13 +565,12 @@
             vm((128, 8, 1024), BF16),
             vm((512, 1024), F32),
             vm((2, TOK, 128), F32),
-            dma((9,)),
+            dma((15,)),
             dma((3,)),
             dma((3,)),
-            dma((5,)),
+            dma((6,)),
+            dma((3,)),
             dma((2,)),
-            dma,
-            dma,
             dma,
             dma,
             dma,

time: 97.7 us -> 95.3 us (0.975)
  Pallas kernels: 96.8 us -> 94.4 us
    pallas_call x1, Pallas kernels: 96.8 us -> 94.4 us  [shards(): pl.pallas_call(kernel, out_shape=jax.ShapeDtypeStruct((TOK, D), BF16), in...]
where the time goes in v3:
time: 95.3 us; the launch traced here: 95.2 us
  Pallas kernels  94.4 us (99%)
    pallas_call x1, Pallas kernels, shards(): pl.pallas_call(kernel, out_shape=jax.ShapeDtypeStruct((TOK, D), BF16), in...  94.4 us

profile of v3, /device:TPU:1, one launch (start us, length us, event | category | flops | bytes accessed | tf_op | source)
XLA Modules:
  0.0 95.2 jit_solution(10411050928829302791)
XLA Ops:
  0.0 94.4 %layer.1 = bf16[128,2048]{1,0:T(8,128)(2,1)S(1)} custom-call(bf16[128,2048]{1,0:T(8,128)(2,1)} %bitcast.22, bf16[128,2048]{1,0:T(8,128)(2,1)} %bitcast.23, bf16[128,2048]{1,0:T(8,128)(2,1)} %bitcast.24, bf16[128,2048]{1,0:T(8,128)(2,1)} %bitcast.25, bf16[2048,256]{1,0:T(8,128)(2,1)} %ow_h.1, bf16[2048,1024]{1,0:T(8,128)(2,1)} %bitcast.19, ...), custom_call_target="tpu_custom_call" | custom-call | tf_op jit(solution)/shard_map/layer/pallas_call | solution.py:531
  94.4 0.8 copy.17

commit v4 on v3

--- a/solution.py
+++ b/solution.py
@@ -368,14 +368,18 @@
     for i in range(blocks):
         weigh(i)
     drain(qkv_r.at[2, pl.ds(0, 15 * TOK)], qkv_recv.at[2])
-    drain(wr.at[pl.ds(0, 256), pl.ds(0, 1024)], w_near.at[1])
-    drain(wr.at[pl.ds(0, 256), pl.ds(0, 1024)], w_near.at[2])
-    relay(512 * (1 - parity), w_send.at[3], w_far.at[1])
 
     def one_block(n, _):
         for i in range(blocks):
             pl.when(block_of(n) == i)(functools.partial(combine, i))
         return_block(block_of(n))
+
+        @pl.when(n == 1)
+        def _():
+            drain(wr.at[pl.ds(0, 256), pl.ds(0, 1024)], w_near.at[1])
+            drain(wr.at[pl.ds(0, 256), pl.ds(0, 1024)], w_near.at[2])
+            relay(512 * (1 - parity), w_send.at[3], w_far.at[1])
+
         return 0
 
     lax.fori_loop(0, blocks, one_block, 0)
@@ -479,12 +483,19 @@
         return 0
 
     lax.fori_loop(0, 4, run_expert, 0)
-    acc[...] = jnp.zeros_like(acc)
-
     def collect(b, _):
         wait_block(ret, r_recv, b)
         rows = ret[pl.ds(pl.multiple_of(b * 32, 32), 32)].reshape(256, 1024)
-        acc[...] += dot(pick[:, pl.ds(pl.multiple_of(b * 256, 256), 256)], rows)
+        picked = dot(pick[:, pl.ds(pl.multiple_of(b * 256, 256), 256)], rows)
+
+        @pl.when(b == 0)
+        def _():
+            acc[...] = picked
+
+        @pl.when(b > 0)
+        def _():
+            acc[...] += picked
+
         return 0
 
     lax.fori_loop(0, 4, collect, 0)

time: 95.3 us -> 95.1 us (level)
  no operation moved by 1% of the time
where the time goes in v4:
time: 95.1 us; the launch traced here: 95 us
  Pallas kernels  94.2 us (99%)
    pallas_call x1, Pallas kernels, shards(): pl.pallas_call(kernel, out_shape=jax.ShapeDtypeStruct((TOK, D), BF16), in...  94.2 us

profile of v4, /device:TPU:1, one launch (start us, length us, event | category | flops | bytes accessed | tf_op | source)
XLA Modules:
  0.0 95.0 jit_solution(13839499809836692208)
XLA Ops:
  0.0 94.2 %layer.1 = bf16[128,2048]{1,0:T(8,128)(2,1)S(1)} custom-call(bf16[128,2048]{1,0:T(8,128)(2,1)} %bitcast.22, bf16[128,2048]{1,0:T(8,128)(2,1)} %bitcast.23, bf16[128,2048]{1,0:T(8,128)(2,1)} %bitcast.24, bf16[128,2048]{1,0:T(8,128)(2,1)} %bitcast.25, bf16[2048,256]{1,0:T(8,128)(2,1)} %ow_h.1, bf16[2048,1024]{1,0:T(8,128)(2,1)} %bitcast.19, ...), custom_call_target="tpu_custom_call" | custom-call | tf_op jit(solution)/shard_map/layer/pallas_call | solution.py:542
  94.2 0.8 copy.17
